TPU v7x, 32 devices: a whole 2x2x4 slice. The times are simulated.
32 devices in a mesh: grp: 2 (over y), sp: 4 (over z), dp: 4 (over x, core).
Axes of the slice: x: 2, y: 2, z: 4, core: 2. Of those that a mesh axis runs over, the one named last changes fastest.
Arguments:
- activations: bfloat16 [8, 2048, 2048], P(('grp', 'dp'), 'sp'), parts along dimension 0, may hold values from -6 to 6
- value_weight: bfloat16 [2048, 1024], P('sp', 'dp'), may hold values from -0.125 to 0.125
- gate_weight: bfloat16 [2048, 1024], P('sp', 'dp'), may hold values from -0.125 to 0.125
- conv_taps: float32 [31, 1024], replicated, may hold values from -4 to 4
- conv_bias: float32 [1024], replicated, may hold values from -3 to 3
- norm_gain: float32 [1024], replicated, may hold values from 0.1 to 1.9
- norm_bias: float32 [1024], replicated, may hold values from -3 to 3
- out_weight: bfloat16 [1024, 2048], P('sp', 'dp'), may hold values from -0.1875 to 0.1875
Outputs:
- mixed_out: bfloat16 [8, 2048, 2048], P(('grp', 'dp'), 'sp'), parts along dimension 0
There are 2 independent parts, one for each index of `grp`. A program takes and returns all parts, laid end to end along the dimension named above; an argument that names none is the same for every part. Nothing has to cross between parts.
All inputs are finite; a program needn't handle non-finite values.
Results may differ from a plain program's by a relative error of at most 0.013.
Values may be sent and summed in bfloat16 or wider, within the bound.
A program may use at most 64 MiB of HBM per device.

v0:
```python
import jax
import jax.numpy as jnp
from jax import lax
from jax.sharding import PartitionSpec as P

epsilon = 1e-05


def passed_along(value, axis, steps):
    count = lax.axis_size(axis)
    first, last = (max(0, -steps), min(count, count - steps))
    return lax.ppermute(value, axis, [(source, source + steps) for source in range(first, last)])


def local(
    activations, value_weight, gate_weight, conv_taps, conv_bias, norm_gain, norm_bias, out_weight
):
    tokens = activations[0]
    tok_rows = tokens.shape[0]
    kernel_len = conv_taps.shape[0]
    whole_value, whole_gate = (
        lax.all_gather(value_weight, "sp", axis=0, tiled=True),
        lax.all_gather(gate_weight, "sp", axis=0, tiled=True),
    )
    stacked = jnp.stack([whole_value, whole_gate], axis=0)
    both_rows = jnp.einsum(
        "td,kdc->ktc",
        tokens,
        lax.all_gather(stacked, "dp", axis=2, tiled=True),
        preferred_element_type=jnp.float32,
    )
    value_rows = both_rows[0]
    gate_rows = both_rows[1]
    value_half = value_rows.astype(jnp.bfloat16)
    gate_half = gate_rows.astype(jnp.bfloat16)
    gated_rows = (
        value_half.astype(jnp.float32) * jax.nn.sigmoid(gate_half.astype(jnp.float32))
    ).astype(jnp.bfloat16)
    prior = passed_along(gated_rows[tok_rows - (kernel_len - 1) :], "sp", 1)
    padded = jnp.concatenate([prior, gated_rows], axis=0).astype(jnp.float32)
    conv_sum = jnp.zeros(gated_rows.shape, jnp.float32) + conv_bias[None, :]
    for tap_index in range(kernel_len):
        conv_sum = (
            conv_sum + conv_taps[tap_index][None, :] * padded[tap_index : tap_index + tok_rows]
        )
    mean_row = jnp.mean(conv_sum, axis=-1, keepdims=True)
    centered = conv_sum - mean_row
    spread = jnp.mean(centered * centered, axis=-1, keepdims=True)
    normed = centered * lax.rsqrt(spread + epsilon) * norm_gain[None, :] + norm_bias[None, :]
    swished = jax.nn.silu(normed).astype(jnp.bfloat16)
    whole_output = lax.all_gather(out_weight, "sp", axis=0, tiled=True)
    result = jnp.dot(
        swished,
        lax.all_gather(whole_output, "dp", axis=1, tiled=True),
        preferred_element_type=jnp.float32,
    )
    return result.astype(jnp.bfloat16)[None]


def solution(mesh):
    in_specs = (
        P(("grp", "dp"), "sp", None),
        P("sp", "dp"),
        P("sp", "dp"),
        P(),
        P(),
        P(),
        P(),
        P("sp", "dp"),
    )
    out_specs = P(("grp", "dp"), "sp", None)
    return jax.shard_map(local, mesh=mesh, in_specs=in_specs, out_specs=out_specs, check_vma=False)
```

profile of v0, /device:TPU:0, one launch (start us, length us, event | category | flops | bytes accessed | tf_op | source)
XLA Modules:
  0.0 207.2 jit_solution(12494679978274099827)
XLA Ops:
  6.5 0.0 copy-start
  6.5 0.0 all-gather.6.cloned.1.call-start
  6.5 0.7 all-gather.6.cloned.1.call-update
  7.3 0.0 all-gather.8.cloned.1.call-start
  7.3 0.7 all-gather.8.cloned.1.call-update
  8.0 0.0 all-gather.12.cloned.1.call-start
  8.1 0.7 all-gather.12.cloned.1.call-update
  8.7 0.0 all-gather.10.cloned.1.call-start
  8.8 30.9 %all-gather.6.cloned.1.call-done = bf16[2048,256]{1,0:T(8,128)(2,1)} async-done(((bf16[512,256]{1,0:T(8,128)(2,1)}), bf16[2048,256]{1,0:T(8,128)(2,1)}) %all-gather.6.cloned.1.call-update) | async-done | bytes 1048592 | tf_op jit(solution)/shard_map/all_gather | solution.py:22
  39.6 29.0 %all-gather.8.cloned.1.call-done = bf16[2048,256]{1,0:T(8,128)(2,1)} async-done(((bf16[512,256]{1,0:T(8,128)(2,1)}), bf16[2048,256]{1,0:T(8,128)(2,1)}) %all-gather.8.cloned.1.call-update) | async-done | bytes 1048592 | tf_op jit(solution)/shard_map/all_gather | solution.py:23
  68.6 3.1 %pad_maximum_fusion = bf16[2,2048,256]{2,1,0:T(8,128)(2,1)} fusion(bf16[1,2048,256]{2,1,0:T(8,128)(2,1)} %bitcast.50, bf16[1,2048,256]{2,1,0:T(8,128)(2,1)} %bitcast.49), kind=kLoop, calls=%fused_computation.64 | loop fusion | flops 1048576 | bytes 4194304 | tf_op jit(solution)/shard_map/stack | solution.py:25
  71.7 0.0 copy-start.2
  71.7 0.0 all-gather.10.cloned.1.call-update
  71.7 0.0 all-gather.14.cloned.1.call-start
  71.7 25.8 %all-gather.12.cloned.1.call-done = bf16[1024,512]{1,0:T(8,128)(2,1)} async-done(((bf16[256,512]{1,0:T(8,128)(2,1)}), bf16[1024,512]{1,0:T(8,128)(2,1)}) %all-gather.12.cloned.1.call-update) | async-done | bytes 1048592 | tf_op jit(solution)/shard_map/all_gather | solution.py:51
  97.6 0.0 all-gather.14.cloned.1.call-update
  97.6 0.0 copy-done.2
  97.6 0.1 fusion.44
  97.7 60.0 %all-gather.10.cloned.1.call-done = bf16[2,2048,1024]{2,1,0:T(8,128)(2,1)} async-done(((bf16[2,2048,256]{2,1,0:T(8,128)(2,1)}), bf16[2,2048,1024]{2,1,0:T(8,128)(2,1)}) %all-gather.10.cloned.1.call-update) | async-done | bytes 8388624 | tf_op jit(solution)/shard_map/all_gather | solution.py:29
  157.8 0.0 copy-done
  157.8 8.1 %convert_bitcast_fusion = bf16[2,512,1024]{2,1,0:T(8,128)(2,1)S(1)} fusion(bf16[2,2048,1024]{2,1,0:T(8,128)(2,1)} %all-gather.10.cloned.1.call-done, bf16[1,512,2048]{2,1,0:T(8,128)(2,1)S(1)} %copy-done), kind=kOutput, calls=%fused_computation.68 | convolution fusion | flops 4296015872 | bytes 12582912 | tf_op jit(solution)/shard_map/td,kdc->ktc/dot_general | solution.py:26
  165.8 0.6 multiply_convert_fusion
  166.5 3.4 %collective-permute-start = (bf16[30,1024]{1,0:T(8,128)(2,1)S(1)}, bf16[30,1024]{1,0:T(8,128)(2,1)S(1)}, u32[]{:S(2)}, u32[]{:S(2)}) collective-permute-start(bf16[30,1024]{1,0:T(8,128)(2,1)S(1)} %slice_bitcast_fusion), channel_id=1, source_target_pairs={{0,4},{4,8},{8,12},{1,5},{5,9},{9,13},{2,6},{6,10},{10,14},{3,7},{... | collective-permute-start | bytes 184328 | tf_op jit(solution)/shard_map/ppermute | solution.py:12
  169.9 0.6 fusion.48
  170.5 0.0 copy-start.3
  170.5 1.3 collective-permute-done
  171.8 0.3 maximum_convert_fusion
  172.1 0.0 copy-done.3
  172.1 9.8 %fusion.42 = (f32[512]{0:T(512)S(1)}, f32[512,1024]{1,0:T(8,128)S(1)}) fusion(f32[542,1024]{1,0:T(8,128)S(1)} %maximum_convert_fusion, f32[1024]{0:T(1024)S(1)} %bitcast.61, f32[1024]{0:T(1024)S(1)} %bitcast.62, f32[1024]{0:T(1024)S(1)} %bitcast.64, f32[1024]{0:T(1024)S(1)} %bitcast.65, f32[1024]{0:T(1024)S(1)} %bitcast.66, f32[1024]{0:T(1024)S(1)} %bitcast.67, ...), kind=kLoop, calls=%fused_computation.81 | loop fusion | flops 33029632 | bytes 67241984 | tf_op jit(solution)/shard_map/reduce_sum | solution.py:46
  181.9 0.0 copy-start.1
  181.9 0.0 copy-start.4
  181.9 0.0 copy-start.5
  182.0 1.3 copy-done.1
  183.3 0.3 multiply_reduce_fusion
  183.6 10.0 %all-gather.14.cloned.1.call-done = bf16[1024,2048]{1,0:T(8,128)(2,1)} async-done(((bf16[1024,512]{1,0:T(8,128)(2,1)}), bf16[1024,2048]{1,0:T(8,128)(2,1)}) %all-gather.14.cloned.1.call-update) | async-done | bytes 4194320 | tf_op jit(solution)/shard_map/all_gather | solution.py:54
  193.7 0.0 copy-done.4
  193.7 0.0 copy-done.5
  193.7 7.0 %fusion = bf16[1,512,2048]{2,1,0:T(8,128)(2,1)} fusion(bf16[1024,2048]{1,0:T(8,128)(2,1)} %all-gather.14.cloned.1.call-done, f32[512,1024]{1,0:T(8,128)} %copy-done.1, f32[1024]{0:T(1024)S(1)} %copy-done.4, f32[1024]{0:T(1024)S(1)} %copy-done.5, f32[512]{0:T(512)S(1)} %add_rsqrt_fusion, f32[512]{0:T(512)S(1)} %broadcast_multiply_fusion), kind=kOutput, calls=%fused_computation.1 | convolution fusion | flops 2153250816 | bytes 8400896 | tf_op jit(solution)/shard_map/dot_general | solution.py:52
  (4 shorter events, 0.1 us)
Async XLA Ops:
  6.5 151.2 %copy-start = (bf16[1,512,2048]{2,1,0:T(8,128)(2,1)S(1)}, bf16[1,512,2048]{2,1,0:T(8,128)(2,1)}, u32[]{:S(2)}) copy-start(bf16[1,512,2048]{2,1,0:T(8,128)(2,1)} %param.8) | copy-start | bytes 6291460
  6.5 33.1 %all-gather.6.cloned.1.call-start = ((), (), s32[]{:S(2)}) async-start(), calls=%async_computation | async-start | bytes 1310720 | tf_op jit(solution)/shard_map/all_gather | solution.py:22
  7.3 61.3 %all-gather.8.cloned.1.call-start = ((), (), s32[]{:S(2)}) async-start(), calls=%async_computation.1 | async-start | bytes 1310720 | tf_op jit(solution)/shard_map/all_gather | solution.py:23
  8.0 89.6 %all-gather.12.cloned.1.call-start = ((), (), s32[]{:S(2)}) async-start(), calls=%async_computation.3 | async-start | bytes 1310720 | tf_op jit(solution)/shard_map/all_gather | solution.py:51
  8.7 149.0 %all-gather.10.cloned.1.call-start = ((), (), s32[]{:S(2)}) async-start(), calls=%async_computation.2 | async-start | bytes 10485760 | tf_op jit(solution)/shard_map/all_gather | solution.py:29
  71.7 25.9 %copy-start.2 = (f32[31,1024]{1,0:T(8,128)S(1)}, f32[31,1024]{1,0:T(8,128)}, u32[]{:S(2)}) copy-start(f32[31,1024]{1,0:T(8,128)} %param.11) | copy-start | bytes 380932
  71.7 122.0 %all-gather.14.cloned.1.call-start = ((), (), s32[]{:S(2)}) async-start(), calls=%async_computation.4 | async-start | bytes 5242880 | tf_op jit(solution)/shard_map/all_gather | solution.py:54
  166.5 5.3 %collective-permute-start = (bf16[30,1024]{1,0:T(8,128)(2,1)S(1)}, bf16[30,1024]{1,0:T(8,128)(2,1)S(1)}, u32[]{:S(2)}, u32[]{:S(2)}) collective-permute-start(bf16[30,1024]{1,0:T(8,128)(2,1)S(1)} %slice_bitcast_fusion), channel_id=1, source_target_pairs={{0,4},{4,8},{8,12},{1,5},{5,9},{9,13},{2,6},{6,10},{10,14},{3,7},{... | collective-permute-start | bytes 184328 | tf_op jit(solution)/shard_map/ppermute | solution.py:12
  170.5 1.6 copy-start.3
  181.9 1.3 copy-start.1
  181.9 11.7 %copy-start.4 = (f32[1024]{0:T(1024)S(1)}, f32[1024]{0:T(1024)}, u32[]{:S(2)}) copy-start(f32[1024]{0:T(1024)} %param.14) | copy-start | bytes 12292
  181.9 11.7 %copy-start.5 = (f32[1024]{0:T(1024)S(1)}, f32[1024]{0:T(1024)}, u32[]{:S(2)}) copy-start(f32[1024]{0:T(1024)} %param.13) | copy-start | bytes 12292
Sparse Core Ops, SparseCore 0:
  8.9 30.6 all-gather.5
  41.2 27.3 all-gather.7
  70.2 27.3 all-gather.11
  99.0 58.7 all-gather.9
  159.2 34.4 all-gather.13
where the time goes:
time: 207 us
  waiting for transfers between devices  159 us (77%)
  matrix products  15 us (7%)
  other arithmetic  14.7 us (7%)
  between operations  13.3 us (6%)
  starting transfers between devices  3.55 us (2%)
    all_gather x1, waiting for transfers between devices, local(): lax.all_gather(stacked, 'dp', axis=2, tiled=True)  60 us
    all_gather x1, waiting for transfers between devices, local(): lax.all_gather(value_weight, 'sp', axis=0, tiled=True)  30.9 us
    all_gather x1, waiting for transfers between devices, local(): lax.all_gather(gate_weight, 'sp', axis=0, tiled=True)  29 us
    all_gather x1, waiting for transfers between devices, local(): whole_output = lax.all_gather(out_weight, 'sp', axis=0, tiled=True)  25.8 us
    all_gather x1, waiting for transfers between devices, local(): lax.all_gather(whole_output, 'dp', axis=1, tiled=True)  10 us
    reduce_sum x1, other arithmetic, local(): mean_row = jnp.mean(conv_sum, axis=-1, keepdims=True)  9.83 us
    dot_general x1, matrix products, local(): jnp.einsum('td,kdc->ktc', tokens, lax.all_gather(stacked, 'dp', axis=2, t...  8.06 us
    dot_general x1, matrix products, local(): jnp.dot(swished, lax.all_gather(whole_output, 'dp', axis=1, tiled=True),...  6.96 us
  transfers between devices with their start and end apart: 6, of which 6 were waited for; matrix products, arithmetic and copies ran while one was open for 11% of the time, Pallas kernels for 0%

commit v1 on v0

v1 whole, which is shorter than its diff:
```python
import functools

import jax
import jax.numpy as jnp
from jax import lax
from jax.experimental import pallas as pl
from jax.experimental.pallas import tpu as pltpu
from jax.sharding import PartitionSpec as P

epsilon = 1e-05
MESH = pl.DeviceIdType.MESH
LANES = 128


def kernel(
    cfg, x_ref, v_ref, g_ref, o_ref, taps_ref, bias_ref, gain_ref, shift_ref, out_ref,
    ext, w1, w2, acc, glu, conv, sw, outv, local_sem, halo_sem, send_sem, recv_w, recv_o,
):
    n, nd, T, H, KB, CB, OB, OC, KW, C = (cfg[k] for k in ("n", "nd", "T", "H", "KB", "CB", "OB", "OC", "KW", "C"))
    NW, NO = cfg["NW"], cfg["NO"]
    nx = nd // 2
    SUB = (NW, NO)
    y, z, d = lax.axis_index("grp"), lax.axis_index("sp"), lax.axis_index("dp")
    x, c = d // 2, d % 2
    has_down, has_up = z > 0, z < n - 1
    down, up = (y, jnp.maximum(z - 1, 0), d), (y, jnp.minimum(z + 1, n - 1), d)
    sibling = (y, z, x * 2 + 1 - c)
    across = (1 - y, z, d)
    columns = [lax.rem(x + dx, nx) * 2 + c for dx in range(1, nx)]

    barrier = pltpu.get_barrier_semaphore()

    def hello(target):
        pl.semaphore_signal(barrier, inc=1, device_id=target, device_id_type=MESH)

    own = [
        pltpu.make_async_copy(v_ref, w1.at[d, pl.ds(pl.multiple_of(z * KB, KB), KB), pl.ds(0, CB)], local_sem.at[0]),
        pltpu.make_async_copy(g_ref, w1.at[d, pl.ds(pl.multiple_of(z * KB, KB), KB), pl.ds(CB, CB)], local_sem.at[1]),
        pltpu.make_async_copy(o_ref, w2.at[d, pl.ds(pl.multiple_of(z * OB, OB), OB), :], local_sem.at[2]),
    ]
    rows = [
        pltpu.make_async_copy(x_ref.at[0, :, pl.ds(k * KB, KB)], ext.at[k, pl.ds(H, T), :], local_sem.at[3 + k])
        for k in range(n)
    ]
    for copy in own + rows:
        copy.start()
    pl.when(has_down)(lambda: hello(down))
    pl.when(has_up)(lambda: hello(up))
    hello(sibling)
    hello(across)
    for other in columns:
        hello((y, z, other))
    pl.semaphore_wait(barrier, nx + 1 + has_down.astype(jnp.int32) + has_up.astype(jnp.int32))

    def unit(kind, zz, dd, u):
        if kind == 0:
            size = KB // NW
            return w1.at[dd, pl.ds(pl.multiple_of(zz * KB + u * size, size), size), :]
        size = OB // NO
        return w2.at[dd, pl.ds(pl.multiple_of(zz * OB + u * size, size), size), :]

    def copy_of(kind, zz, dd, u, target):
        ref = unit(kind, zz, dd, u)
        return pltpu.make_async_remote_copy(
            src_ref=ref, dst_ref=ref, send_sem=send_sem.at[kind],
            recv_sem=(recv_w, recv_o)[kind].at[zz, dd, u], device_id=target, device_id_type=MESH,
        )

    def arrive(kind, zz, dd, u, drain):
        if not drain:
            copy_of(kind, zz, dd, u, sibling).wait_recv()

    def send(kind, zz, dd, u, target, drain):
        copy = copy_of(kind, zz, dd, u, target)
        copy.wait_send() if drain else copy.start()

    def both_ways(kind, e, body):
        sub = SUB[kind]
        r, u = e // sub, e % sub
        for sgn in (1, -1):
            zz = z + sgn * r
            valid = (zz >= 0) & (zz < n) & (r >= 0) & (r < n) & (e >= 0)
            if sgn == -1:
                valid = valid & (r > 0)
            pl.when(valid)(functools.partial(body, zz, r, u, sgn))

    def event_z(kind, e, drain=False):
        def body(zz, r, u, sgn):
            pl.when(r > 0)(lambda: arrive(kind, zz, d, u, drain))
            to_down = has_down if sgn == 1 else has_down & (r == 0)
            to_up = has_up & (r == 0) if sgn == 1 else has_up
            pl.when(to_down)(lambda: send(kind, zz, d, u, down, drain))
            pl.when(to_up)(lambda: send(kind, zz, d, u, up, drain))

            @pl.when(u % 2 == y)
            def _():
                for other in columns:
                    send(kind, zz, d, u, (y, z, other), drain)

            send(kind, zz, d, u, sibling, drain)

        both_ways(kind, e, body)

    def event_x(kind, e, drain=False):
        def body(zz, r, u, sgn):
            @pl.when(u % 2 == y)
            def _():
                for other in columns:
                    arrive(kind, zz, other, u, drain)
                    send(kind, zz, other, u, across, drain)
                    send(kind, zz, other, u, sibling, drain)

        both_ways(kind, e, body)

    def event_y(kind, e, drain=False):
        def body(zz, r, u, sgn):
            @pl.when(u % 2 != y)
            def _():
                for other in columns:
                    arrive(kind, zz, other, u, drain)
                    send(kind, zz, other, u, sibling, drain)

        both_ways(kind, e, body)

    def event_sibling(kind, e):
        def body(zz, r, u, sgn):
            for xx in range(nx):
                arrive(kind, zz, xx * 2 + 1 - c, u, False)

        both_ways(kind, e, body)

    def project(e):
        def body(zz, r, u, sgn):
            @pl.when(u == NW - 1)
            def _():
                def column(dd, _):
                    block = w1[dd, pl.ds(pl.multiple_of(zz * KB, KB), KB), :]
                    acc[dd] += jnp.dot(ext[zz], block, preferred_element_type=jnp.float32)
                    return 0

                lax.fori_loop(0, nd, column, 0)

        both_ways(0, e, body)

    halo = pltpu.make_async_remote_copy(
        src_ref=ext.at[:, pl.ds(T, H), :],
        dst_ref=ext.at[:, pl.ds(0, H), :],
        send_sem=halo_sem.at[0], recv_sem=halo_sem.at[1], device_id=up, device_id_type=MESH,
    )
    own[0].wait()
    own[1].wait()

    def first(e, _):
        event_z(0, e)
        return 0

    lax.fori_loop(0, NW, first, 0)
    for copy in rows:
        copy.wait()
    pl.when(has_up)(lambda: halo.start())
    own[2].wait()

    @pl.when(z == 0)
    def _():
        ext[:, 0:H, :] = jnp.zeros((n, H, KB), ext.dtype)

    def clear(dd, _):
        acc[dd] = jnp.zeros(acc.shape[1:], jnp.float32)
        return 0

    lax.fori_loop(0, nd, clear, 0)
    pl.when(has_down)(lambda: halo.wait_recv())

    def rest_of_step(e):
        event_x(0, e - cfg["LX"])
        event_y(0, e - cfg["LY"])
        event_sibling(0, e - cfg["LS"])
        project(e - cfg["LS"])

    def step(e, _):
        pl.when(e >= NW)(lambda: event_z(0, e))
        rest_of_step(e)
        return 0

    lax.fori_loop(0, n * NW, step, 0)

    def first_out(e, _):
        event_z(1, e)
        return 0

    lax.fori_loop(0, NO, first_out, 0)

    def last_steps(e, _):
        rest_of_step(e)
        return 0

    lax.fori_loop(n * NW, n * NW + cfg["LS"], last_steps, 0)

    GR = H
    per = CB // LANES

    def gate(i, _):
        at = pl.ds(pl.multiple_of(i * GR, GR), GR)
        for dd in range(nd):
            gated = acc[dd, at, 0:CB] * jax.nn.sigmoid(acc[dd, at, CB : 2 * CB])
            for p in range(per):
                glu[dd * per + p, at, :] = gated[:, p * LANES : (p + 1) * LANES]
        return 0

    lax.fori_loop(0, (T + H) // GR, gate, 0)

    R = cfg["R"]
    tiles = C // LANES
    offset = H - (KW - 1)
    reach = (offset + KW - 1) // 8 * 8

    def rows_of(i):
        base = pl.multiple_of(i * R, R)

        def channel(ct, total):
            lanes = pl.ds(pl.multiple_of(ct * LANES, LANES), LANES)
            block = glu[ct, pl.ds(base, R + H), :]
            block = jnp.concatenate([block, jnp.zeros((8, LANES), jnp.float32)], axis=0)
            value = jnp.broadcast_to(bias_ref[:, lanes], (R, LANES))
            for b in range(8):
                part = None
                for q in range(b, offset + KW, 8):
                    if q < offset:
                        continue
                    start = q - b
                    term = taps_ref[pl.ds(q - offset, 1), lanes] * block[start : start + R + 8]
                    part = term if part is None else part + term
                if part is not None:
                    value = value + part[b : b + R]
            conv[ct] = value
            return total + value

        total = lax.fori_loop(0, tiles, channel, jnp.zeros((R, LANES), jnp.float32))
        mean = jnp.sum(total, axis=-1, keepdims=True) * (1.0 / C)
        square = jnp.zeros((R, LANES), jnp.float32)
        for ct in range(tiles):
            centred = conv[ct] - mean
            square = square + centred * centred
        scale = lax.rsqrt(jnp.sum(square, axis=-1, keepdims=True) * (1.0 / C) + epsilon)
        for ct in range(tiles):
            lanes = slice(ct * LANES, (ct + 1) * LANES)
            normed = (conv[ct] - mean) * scale * gain_ref[:, lanes] + shift_ref[:, lanes]
            sw[pl.ds(base, R), lanes] = (normed * jax.nn.sigmoid(normed)).astype(sw.dtype)

    def out_step(e):
        pl.when(e >= NO)(lambda: event_z(1, e))
        event_x(1, e - 1)
        event_y(1, e - 2)
        event_sibling(1, e - 3)

    row_tiles = T // R
    out_steps = n * NO + 3

    def mixed(i, _):
        pl.when(i < row_tiles)(lambda: rows_of(i))
        pl.when(i < out_steps)(lambda: out_step(i))
        return 0

    lax.fori_loop(0, max(row_tiles, out_steps), mixed, 0)

    for dd in range(nd):
        outv[dd] = jnp.dot(sw[...], w2[dd], preferred_element_type=jnp.float32).astype(outv.dtype)
        pltpu.make_async_copy(outv.at[dd], out_ref.at[0, :, pl.ds(dd * OC, OC)], local_sem.at[dd]).start()

    pl.when(has_up)(lambda: halo.wait_send())
    for kind in (0, 1):
        def drain(e, _, kind=kind):
            event_z(kind, e, True)
            event_x(kind, e, True)
            event_y(kind, e, True)
            return 0

        lax.fori_loop(0, n * SUB[kind], drain, 0)
    for dd in range(nd):
        pltpu.make_async_copy(outv.at[dd], out_ref.at[0, :, pl.ds(dd * OC, OC)], local_sem.at[dd]).wait()


def local(activations, value_weight, gate_weight, conv_taps, conv_bias, norm_gain, norm_bias, out_weight):
    n, nd = lax.axis_size("sp"), lax.axis_size("dp")
    _, T, D = activations.shape
    KB, CB = value_weight.shape
    OB, OC = out_weight.shape
    KW, C = conv_taps.shape
    H = -(-(KW - 1) // 16) * 16
    NW = max(2, min(4, KB // 64))
    NO = 2
    cfg = dict(n=n, nd=nd, T=T, H=H, KB=KB, CB=CB, OB=OB, OC=OC, KW=KW, C=C, NW=NW, NO=NO, R=64, LX=2, LY=4, LS=5)
    anywhere = pl.BlockSpec(memory_space=pl.ANY)
    vmem = pl.BlockSpec(memory_space=pltpu.VMEM)
    bf16, f32 = jnp.bfloat16, jnp.float32
    return pl.pallas_call(
        functools.partial(kernel, cfg),
        out_shape=jax.ShapeDtypeStruct((1, T, D), bf16),
        in_specs=[anywhere] * 4 + [vmem] * 4,
        out_specs=anywhere,
        scratch_shapes=[
            pltpu.VMEM((n, T + H, KB), bf16),
            pltpu.VMEM((nd, n * KB, 2 * CB), bf16),
            pltpu.VMEM((nd, n * OB, OC), bf16),
            pltpu.VMEM((nd, T + H, 2 * CB), f32),
            pltpu.VMEM((C // LANES, T + H, LANES), f32),
            pltpu.VMEM((C // LANES, 64, LANES), f32),
            pltpu.VMEM((T, C), bf16),
            pltpu.VMEM((nd, T, OC), bf16),
            pltpu.SemaphoreType.DMA((max(nd, 3 + n),)),
            pltpu.SemaphoreType.DMA((2,)),
            pltpu.SemaphoreType.DMA((2,)),
            pltpu.SemaphoreType.DMA((n, nd, NW)),
            pltpu.SemaphoreType.DMA((n, nd, NO)),
        ],
        compiler_params=pltpu.CompilerParams(collective_id=0, has_side_effects=True, vmem_limit_bytes=56 * 2**20),
    )(
        activations, value_weight, gate_weight, out_weight,
        conv_taps, conv_bias[None], norm_gain[None], norm_bias[None],
    )


def solution(mesh):
    in_specs = (P(("grp", "dp"), "sp", None), P("sp", "dp"), P("sp", "dp"), P(), P(), P(), P(), P("sp", "dp"))
    out_specs = P(("grp", "dp"), "sp", None)
    return jax.shard_map(local, mesh=mesh, in_specs=in_specs, out_specs=out_specs, check_vma=False)
```

time: 207 us -> 94.2 us (0.46)
  waiting for transfers between devices: 159 us -> 0 us
  Pallas kernels: 0 us -> 90.1 us
  matrix products: 15 us -> 0 us
  other arithmetic: 14.7 us -> 0 us
  between operations: 13.3 us -> 0.01 us
  starting transfers between devices: 3.55 us -> 0 us
    all_gather x5 -> x0, waiting for transfers between devices: 156 us -> none  [the longest x1 60 us: local(): lax.all_gather(stacked, 'dp', axis=2, tiled=True)]
    pallas_call x0 -> x1, Pallas kernels: none -> 90.1 us  [local(): pl.pallas_call(functools.partial(kernel, cfg), out_shape=jax.ShapeDtypeSt...]
    dot_general x2 -> x0, matrix products: 15 us -> none  [the longest x1 8.06 us: local(): jnp.einsum('td,kdc->ktc', tokens, lax.all_gather(stacked, 'dp', axis=2, t...]
    reduce_sum x2 -> x0, other arithmetic: 10.2 us -> none  [the longest x1 9.83 us: local(): mean_row = jnp.mean(conv_sum, axis=-1, keepdims=True)]
    ppermute x1 -> x0, starting transfers between devices: 3.39 us -> none  [passed_along(): lax.ppermute(value, axis, [(source, source + steps) for source in range(f...]
    another operation x1 -> x0, other arithmetic: 3.05 us -> none  [local(): stacked = jnp.stack([whole_value, whole_gate], axis=0)]
    unnamed x5 -> x0, waiting for transfers between devices: 2.12 us -> none
  transfers between devices with their start and end apart: 6 -> 0, of which waited for: 6 -> 0; matrix products, arithmetic and copies ran while one was open for 11% -> 0% of each run, Pallas kernels for 0% -> 0%
where the time goes in v1:
time: 94.2 us; the launch traced here: 93.2 us
  Pallas kernels  90.1 us (96%)
  local copies, waits for them, and re-layouts  3.16 us (3%)
    pallas_call x1, Pallas kernels, local(): pl.pallas_call(functools.partial(kernel, cfg), out_shape=jax.ShapeDtypeSt...  90.1 us
    unnamed x1, local copies, waits for them, and re-layouts  3.16 us

profile of v1, /device:TPU:0, one launch (start us, length us, event | category | flops | bytes accessed | tf_op | source)
XLA Modules:
  0.0 93.2 jit_solution(16175985273041839170)
XLA Ops:
  0.0 90.1 %shard_map.82 = bf16[1,512,2048]{2,1,0:T(8,128)(2,1)} custom-call(bf16[1,512,2048]{2,1,0:T(8,128)(2,1)} %x_ref.1, bf16[512,256]{1,0:T(8,128)(2,1)} %v_ref.1, bf16[512,256]{1,0:T(8,128)(2,1)} %g_ref.1, bf16[256,512]{1,0:T(8,128)(2,1)} %o_ref.1, f32[31,1024]{1,0:T(8,128)} %taps_ref.1, f32[1,1024]{1,0:T(1,128)} %bitcast.3, f32[1,1024]{1,0:T(1,128)} %bitcast.4, ...), custom_call_target="tpu_custom_call" | custom-call | tf_op jit(solution)/shard_map/pallas_call | solution.py:296
  90.1 3.2 %copy.10 = bf16[1,512,2048]{2,1,0:T(8,128)(2,1)} copy(bf16[1,512,2048]{2,1,0:T(8,128)(2,1)} %shard_map.82) | data formatting | bytes 4194304

commit v2 on v1

--- a/solution.py
+++ b/solution.py
@@ -20,6 +20,7 @@
     NW, NO = cfg["NW"], cfg["NO"]
     nx = nd // 2
     SUB = (NW, NO)
+    GROUP = (max(1, NW // 2), max(1, NO // 2))
     y, z, d = lax.axis_index("grp"), lax.axis_index("sp"), lax.axis_index("dp")
     x, c = d // 2, d % 2
     has_down, has_up = z > 0, z < n - 1
@@ -84,61 +85,106 @@
                 valid = valid & (r > 0)
             pl.when(valid)(functools.partial(body, zz, r, u, sgn))
 
+    at_end = (z == 0) | (z == n - 1)
+
+    def skipped(kind, r, u, plane):
+        return (u % 2 != plane) & ((u // 2 % 2 == 0) | (kind == 0)) & (r < n - 1 if kind == 0 else r < n - 2)
+
+    def both_planes(kind, r):
+        return r >= (n if kind == 0 else n - 2)
+
+    def direct(kind, r, u):
+        return (u % 2 == y) | both_planes(kind, r)
+
     def event_z(kind, e, drain=False):
         def body(zz, r, u, sgn):
-            pl.when(r > 0)(lambda: arrive(kind, zz, d, u, drain))
-            to_down = has_down if sgn == 1 else has_down & (r == 0)
-            to_up = has_up & (r == 0) if sgn == 1 else has_up
-            pl.when(to_down)(lambda: send(kind, zz, d, u, down, drain))
-            pl.when(to_up)(lambda: send(kind, zz, d, u, up, drain))
-
-            @pl.when(u % 2 == y)
-            def _():
-                for other in columns:
-                    send(kind, zz, d, u, (y, z, other), drain)
-
-            send(kind, zz, d, u, sibling, drain)
+            detour = at_end & (r > 0)
+
+            @pl.when(jnp.logical_not(detour & skipped(kind, r, u, y)))
+            def _():
+                pl.when(r > 0)(lambda: arrive(kind, zz, d, u, drain))
+                to_down = has_down if sgn == 1 else has_down & (r == 0)
+                to_up = has_up & (r == 0) if sgn == 1 else has_up
+                to_down = to_down & jnp.logical_not((z == 1) & skipped(kind, r + 1, u, y))
+                to_up = to_up & jnp.logical_not((z == n - 2) & skipped(kind, r + 1, u, y))
+                pl.when(to_down)(lambda: send(kind, zz, d, u, down, drain))
+                pl.when(to_up)(lambda: send(kind, zz, d, u, up, drain))
+                pl.when(detour & skipped(kind, r, u, 1 - y))(lambda: send(kind, zz, d, u, across, drain))
+
+                @pl.when(direct(kind, r, u))
+                def _():
+                    for other in columns:
+                        send(kind, zz, d, u, (y, z, other), drain)
 
         both_ways(kind, e, body)
 
     def event_x(kind, e, drain=False):
         def body(zz, r, u, sgn):
-            @pl.when(u % 2 == y)
+            @pl.when(direct(kind, r, u))
             def _():
                 for other in columns:
                     arrive(kind, zz, other, u, drain)
-                    send(kind, zz, other, u, across, drain)
-                    send(kind, zz, other, u, sibling, drain)
+                    pl.when(jnp.logical_not(both_planes(kind, r)))(
+                        functools.partial(send, kind, zz, other, u, across, drain)
+                    )
 
         both_ways(kind, e, body)
 
     def event_y(kind, e, drain=False):
         def body(zz, r, u, sgn):
-            @pl.when(u % 2 != y)
+            @pl.when(jnp.logical_not(direct(kind, r, u)))
             def _():
                 for other in columns:
                     arrive(kind, zz, other, u, drain)
-                    send(kind, zz, other, u, sibling, drain)
+
+            @pl.when(at_end & (r > 0) & skipped(kind, r, u, y))
+            def _():
+                arrive(kind, zz, d, u, drain)
+
+        both_ways(kind, e, body)
+
+    def group_of(kind, zz, dd, u):
+        size = (KB // NW, OB // NO)[kind]
+        many = GROUP[kind]
+        first_row = zz * size * SUB[kind] + (u - many + 1) * size
+        ref = (w1, w2)[kind].at[dd, pl.ds(pl.multiple_of(first_row, size * many), size * many), :]
+        return pltpu.make_async_remote_copy(
+            src_ref=ref, dst_ref=ref, send_sem=send_sem.at[kind],
+            recv_sem=(recv_w, recv_o)[kind].at[zz, dd, u], device_id=sibling, device_id_type=MESH,
+        )
+
+    def event_hand(kind, e, drain=False):
+        def body(zz, r, u, sgn):
+            @pl.when(u % GROUP[kind] == GROUP[kind] - 1)
+            def _():
+                for xx in range(nx):
+                    copy = group_of(kind, zz, xx * 2 + c, u)
+                    copy.wait_send() if drain else copy.start()
 
         both_ways(kind, e, body)
 
     def event_sibling(kind, e):
         def body(zz, r, u, sgn):
-            for xx in range(nx):
-                arrive(kind, zz, xx * 2 + 1 - c, u, False)
+            @pl.when(u % GROUP[kind] == GROUP[kind] - 1)
+            def _():
+                for xx in range(nx):
+                    group_of(kind, zz, xx * 2 + 1 - c, u).wait_recv()
 
         both_ways(kind, e, body)
 
     def project(e):
         def body(zz, r, u, sgn):
-            @pl.when(u == NW - 1)
-            def _():
-                def column(dd, _):
+            per_step = -(-nd // NW)
+
+            @pl.when(u * per_step < nd)
+            def _():
+                def column(k, _):
+                    dd = u * per_step + k
                     block = w1[dd, pl.ds(pl.multiple_of(zz * KB, KB), KB), :]
                     acc[dd] += jnp.dot(ext[zz], block, preferred_element_type=jnp.float32)
                     return 0
 
-                lax.fori_loop(0, nd, column, 0)
+                lax.fori_loop(0, per_step, column, 0)
 
         both_ways(0, e, body)
 
@@ -171,30 +217,42 @@
     lax.fori_loop(0, nd, clear, 0)
     pl.when(has_down)(lambda: halo.wait_recv())
 
-    def rest_of_step(e):
-        event_x(0, e - cfg["LX"])
-        event_y(0, e - cfg["LY"])
-        event_sibling(0, e - cfg["LS"])
-        project(e - cfg["LS"])
-
-    def step(e, _):
+    EW, EO = n * NW, n * NO
+    LX, LY, LS = cfg["LX"], cfg["LY"], cfg["LS"]
+    MX, MY, MS = cfg["MX"], cfg["MY"], cfg["MS"]
+    EARLY = cfg["EARLY"] * NW
+
+    def weights_rest(e):
+        event_x(0, e - LX)
+        event_y(0, e - LY)
+        event_hand(0, e - LY)
+        event_sibling(0, e - LS)
+        project(e - LS - NW + 1)
+
+    def out_step(e):
+        pl.when(e >= NO)(lambda: event_z(1, e))
+        event_x(1, e - MX)
+        event_y(1, e - MY)
+        event_hand(1, e - MY)
+        event_sibling(1, e - MS)
+
+    def weights_step(e, _):
+        pl.when((e >= EARLY) & (e < EARLY + NO))(lambda: event_z(1, e - EARLY))
         pl.when(e >= NW)(lambda: event_z(0, e))
-        rest_of_step(e)
-        return 0
-
-    lax.fori_loop(0, n * NW, step, 0)
-
-    def first_out(e, _):
-        event_z(1, e)
-        return 0
-
-    lax.fori_loop(0, NO, first_out, 0)
-
-    def last_steps(e, _):
-        rest_of_step(e)
-        return 0
-
-    lax.fori_loop(n * NW, n * NW + cfg["LS"], last_steps, 0)
+        weights_rest(e)
+        return 0
+
+    lax.fori_loop(0, EW, weights_step, 0)
+    tail = LS + NW - 1
+    ahead = max(0, n - 2) * NO
+
+    def tail_step(t, _):
+        pl.when((t % 2 == 1) & (t // 2 < ahead))(lambda: out_step(NO + t // 2))
+        weights_rest(EW + t)
+        return 0
+
+    lax.fori_loop(0, tail, tail_step, 0)
+    done = NO + min(ahead, tail // 2)
 
     GR = H
     per = CB // LANES
@@ -247,35 +305,36 @@
             normed = (conv[ct] - mean) * scale * gain_ref[:, lanes] + shift_ref[:, lanes]
             sw[pl.ds(base, R), lanes] = (normed * jax.nn.sigmoid(normed)).astype(sw.dtype)
 
-    def out_step(e):
-        pl.when(e >= NO)(lambda: event_z(1, e))
-        event_x(1, e - 1)
-        event_y(1, e - 2)
-        event_sibling(1, e - 3)
+    def drain(kind, e, _):
+        event_z(kind, e, True)
+        event_x(kind, e, True)
+        event_y(kind, e, True)
+        event_hand(kind, e, True)
+        return 0
 
     row_tiles = T // R
-    out_steps = n * NO + 3
+    drained = -(-EW // row_tiles)
+    each = -(-(EO + MS - done) // row_tiles)
 
     def mixed(i, _):
-        pl.when(i < row_tiles)(lambda: rows_of(i))
-        pl.when(i < out_steps)(lambda: out_step(i))
-        return 0
-
-    lax.fori_loop(0, max(row_tiles, out_steps), mixed, 0)
+        rows_of(i)
+
+        def one(k, _):
+            out_step(done + i * each + k)
+            return 0
+
+        lax.fori_loop(0, each, one, 0)
+        lax.fori_loop(i * drained, (i + 1) * drained, functools.partial(drain, 0), 0)
+        return 0
+
+    lax.fori_loop(0, row_tiles, mixed, 0)
 
     for dd in range(nd):
         outv[dd] = jnp.dot(sw[...], w2[dd], preferred_element_type=jnp.float32).astype(outv.dtype)
         pltpu.make_async_copy(outv.at[dd], out_ref.at[0, :, pl.ds(dd * OC, OC)], local_sem.at[dd]).start()
 
     pl.when(has_up)(lambda: halo.wait_send())
-    for kind in (0, 1):
-        def drain(e, _, kind=kind):
-            event_z(kind, e, True)
-            event_x(kind, e, True)
-            event_y(kind, e, True)
-            return 0
-
-        lax.fori_loop(0, n * SUB[kind], drain, 0)
+    lax.fori_loop(0, EO, functools.partial(drain, 1), 0)
     for dd in range(nd):
         pltpu.make_async_copy(outv.at[dd], out_ref.at[0, :, pl.ds(dd * OC, OC)], local_sem.at[dd]).wait()
 
@@ -287,9 +346,9 @@
     OB, OC = out_weight.shape
     KW, C = conv_taps.shape
     H = -(-(KW - 1) // 16) * 16
-    NW = max(2, min(4, KB // 64))
-    NO = 2
-    cfg = dict(n=n, nd=nd, T=T, H=H, KB=KB, CB=CB, OB=OB, OC=OC, KW=KW, C=C, NW=NW, NO=NO, R=64, LX=2, LY=4, LS=5)
+    NW = max(2, min(8, KB // 64))
+    NO = max(2, min(4, OB // 64))
+    cfg = dict(n=n, nd=nd, T=T, H=H, KB=KB, CB=CB, OB=OB, OC=OC, KW=KW, C=C, NW=NW, NO=NO, R=64, LX=4, LY=10, LS=12, MX=4, MY=7, MS=9, EARLY=min(3, n - 1))
     anywhere = pl.BlockSpec(memory_space=pl.ANY)
     vmem = pl.BlockSpec(memory_space=pltpu.VMEM)
     bf16, f32 = jnp.bfloat16, jnp.float32

time: 94.2 us -> 80.8 us (0.86)
  Pallas kernels: 90.1 us -> 76.9 us
    pallas_call x1, Pallas kernels: 90.1 us -> 76.9 us  [local(): pl.pallas_call(functools.partial(kernel, cfg), out_shape=jax.ShapeDtypeSt...]
where the time goes in v2:
time: 80.8 us; the launch traced here: 80.1 us
  Pallas kernels  76.9 us (95%)
  local copies, waits for them, and re-layouts  3.16 us (4%)
    pallas_call x1, Pallas kernels, local(): pl.pallas_call(functools.partial(kernel, cfg), out_shape=jax.ShapeDtypeSt...  76.9 us
    unnamed x1, local copies, waits for them, and re-layouts  3.16 us

profile of v2, /device:TPU:0, one launch (start us, length us, event | category | flops | bytes accessed | tf_op | source)
XLA Modules:
  0.0 80.1 jit_solution(1676294999350475006)
XLA Ops:
  0.0 76.9 %shard_map.82 = bf16[1,512,2048]{2,1,0:T(8,128)(2,1)} custom-call(bf16[1,512,2048]{2,1,0:T(8,128)(2,1)} %x_ref.1, bf16[512,256]{1,0:T(8,128)(2,1)} %v_ref.1, bf16[512,256]{1,0:T(8,128)(2,1)} %g_ref.1, bf16[256,512]{1,0:T(8,128)(2,1)} %o_ref.1, f32[31,1024]{1,0:T(8,128)} %taps_ref.1, f32[1,1024]{1,0:T(1,128)} %bitcast.3, f32[1,1024]{1,0:T(1,128)} %bitcast.4, ...), custom_call_target="tpu_custom_call" | custom-call | tf_op jit(solution)/shard_map/pallas_call | solution.py:355
  76.9 3.2 %copy.10 = bf16[1,512,2048]{2,1,0:T(8,128)(2,1)} copy(bf16[1,512,2048]{2,1,0:T(8,128)(2,1)} %shard_map.82) | data formatting | bytes 4194304
